TPU v7x, 32 devices: a whole 2x2x4 slice. The times are simulated.
32 devices in a mesh: ra: 8 (over z, y), cb: 4 (over x, core).
Axes of the slice: x: 2, y: 2, z: 4, core: 2. Of those that a mesh axis runs over, the one named last changes fastest.
Arguments:
- tokens: bfloat16 [512, 4096], P(None, 'cb'), may hold values from -82 to 82
- gate_weight: float32 [2, 4096, 11264], P(None, 'cb', 'ra'), may hold values from -0.09375 to 0.09375
- up_weight: float32 [2, 4096, 11264], P(None, 'cb', 'ra'), may hold values from -0.09375 to 0.09375
- down_weight: float32 [2, 11264, 4096], P(None, 'ra', 'cb'), may hold values from -0.0546875 to 0.0546875
- gate_scale: float32 [2, 11264], P(None, 'ra'), may hold values from 0.5 to 2
- up_scale: float32 [2, 11264], P(None, 'ra'), may hold values from 0.5 to 2
- down_scale: float32 [2, 4096], P(None, 'cb'), may hold values from 0.5 to 2
- norm_gain: float32 [2, 4096], P(None, 'cb'), may hold values from 0.1 to 1.9
- conv_taps: float32 [2, 3, 11264], P(None, None, 'ra'), may hold values from -3 to 3
- conv_bias: float32 [2, 11264], P(None, 'ra'), may hold values from -3 to 3
Outputs:
- layer_out: bfloat16 [512, 4096], P(None, 'cb')
All inputs are finite; a program needn't handle non-finite values.
Results may differ from a plain program's by a relative error of at most 0.012.
Values may be sent and summed in bfloat16 or wider, within the bound.
A program may use at most 128 MiB of HBM per device.

v0:
```python
import functools

import jax
import jax.numpy as jnp
from jax import lax
from jax.experimental import pallas as pl
from jax.experimental.pallas import tpu as pltpu
from jax.sharding import PartitionSpec as P

MESH = pl.DeviceIdType.MESH
norm_eps = 1e-06
residual_scale = 0.25
LANES = 128
LAG = 3
CHUNKS = 2


def kernel(
    sizes,
    tok,
    gw_hbm,
    uw_hbm,
    dw_hbm,
    gs,
    us,
    ds_,
    gain,
    taps,
    bias,
    out,
    gw,
    uw,
    dw,
    dwb,
    operand,
    rsb,
    stat,
    part,
    crecv,
    xsend,
    xrecv,
    hid,
    ysend,
    own,
    yrecv,
    zsend,
    zrecv,
    hnew,
    wsem,
    ssem,
    csem,
    xsem,
    hsem,
    ysem,
    zsem,
    asem,
    fsem,
):
    layers, n_tok, d_loc, f_loc, d_all, n_z = sizes
    tiles = f_loc // LANES
    span = n_tok // CHUNKS
    half, quarter = span // 2, span // 4
    zrows = half // n_z
    f32, bf16 = jnp.float32, jnp.bfloat16
    ra, cb = lax.axis_index("ra"), lax.axis_index("cb")
    z, y = ra // 2, ra % 2
    x, c = cb // 2, cb % 2
    core_dev = (ra, x * 2 + (1 - c))
    x_dev = (ra, (1 - x) * 2 + c)
    y_dev = (z * 2 + (1 - y), cb)

    def z_dev(k):
        return (lax.rem(z + k, n_z) * 2 + y, cb)

    def remote(src, dst, sems, dev):
        return pltpu.make_async_remote_copy(
            src_ref=src, dst_ref=dst, send_sem=sems[0], recv_sem=sems[1], device_id=dev, device_id_type=MESH
        )

    def load(l, n):
        src, dst = ((gw_hbm, gw), (uw_hbm, uw), (dw_hbm, dw))[n]
        return pltpu.make_async_copy(src.at[l], dst.at[l], wsem.at[l, n])

    load(0, 0).start()
    load(0, 1).start()

    barrier = pltpu.get_barrier_semaphore()
    peers = [(ra, lax.rem(cb + k, 4)) for k in range(1, 4)] + [y_dev] + [z_dev(k) for k in range(1, n_z)]
    for dev in peers:
        pl.semaphore_signal(barrier, inc=1, device_id=dev, device_id_type=MESH)
    pl.semaphore_wait(barrier, len(peers))

    def block_rows(ch, cc, xx):
        return pl.ds(pl.multiple_of(ch * span + cc * half + xx * quarter, quarter), quarter)

    def zr(zz):
        return pl.ds(pl.multiple_of(zz * zrows, zrows), zrows)

    def hr(ch, yy, zz):
        return pl.ds(pl.multiple_of(ch * span + yy * half + zz * zrows, zrows), zrows)

    for l in range(layers):
        h = tok if l == 0 else hnew.at[l - 1]
        wide = h[...].astype(f32)
        ssq = jnp.sum(wide * wide, axis=1, keepdims=True)
        lane = lax.broadcasted_iota(jnp.int32, (n_tok, LANES), 1)
        row = lax.broadcasted_iota(jnp.int32, (n_tok, LANES), 0)
        pick = lane == lax.shift_right_logical(row, 3)
        packed = jnp.where(pick, jnp.broadcast_to(ssq, (n_tok, LANES)), 0.0)
        stat[l, 0] = jnp.sum(packed.reshape(n_tok // 8, 8, LANES), axis=0)
        for k in range(1, 4):
            remote(
                stat.at[l, 0], stat.at[l, k], (ssem.at[0, l, k - 1], ssem.at[1, l, k - 1]), (ra, lax.rem(cb + k, 4))
            ).start()
        operand[...] = (h[...].astype(f32) * gain[l : l + 1, :]).astype(bf16)
        if l == 0:
            load(0, 0).wait()
            load(0, 1).wait()
            load(0, 2).start()
            for ll in range(1, layers):
                for n in range(3):
                    load(ll, n).start()
        else:
            load(l, 0).wait()
            load(l, 1).wait()
        for k in range(1, 4):
            remote(
                stat.at[l, 0], stat.at[l, k], (ssem.at[0, l, k - 1], ssem.at[1, l, k - 1]), (ra, lax.rem(cb + k, 4))
            ).wait()
        total = stat[l, 0] + stat[l, 1] + stat[l, 2] + stat[l, 3]
        spread = jnp.broadcast_to(total[None], (n_tok // 8, 8, LANES)).reshape(n_tok, LANES)
        summed = jnp.sum(jnp.where(pick, spread, 0.0), axis=1, keepdims=True)
        rsb[...] = jnp.broadcast_to(lax.rsqrt(summed / d_all + norm_eps), (n_tok, LANES))

        def core_copy(ch, j):
            rows = pl.ds(pl.multiple_of(ch * span + (1 - c) * half, half), half)
            return remote(
                part.at[j, rows, :], crecv.at[l, ch, j], (csem.at[0, l, ch, j], csem.at[1, l, ch, j]), core_dev
            )

        def x_copy(ch, j):
            return remote(xsend.at[ch, j], xrecv.at[l, ch, j], (xsem.at[0, l, ch, j], xsem.at[1, l, ch, j]), x_dev)

        x_local = pl.ds(pl.multiple_of((1 - x) * quarter, quarter), quarter)
        m_local = pl.ds(pl.multiple_of(x * quarter, quarter), quarter)

        def x_step(ch, i):
            core_copy(ch, i).wait_recv()
            xsend[ch, i] = (
                part[i, block_rows(ch, c, 1 - x), :].astype(f32) + crecv[l, ch, i, x_local, :].astype(f32)
            ).astype(bf16)
            x_copy(ch, i).start()

        def gate_step(j, carry):
            @pl.when(j < tiles)
            def _():
                cols = pl.ds(pl.multiple_of(j * LANES, LANES), LANES)
                w = jnp.concatenate([gw[l, :, cols].astype(bf16), uw[l, :, cols].astype(bf16)], axis=1)
                acc = jnp.dot(operand[...], w, preferred_element_type=f32)
                rs = rsb[...]
                g = acc[:, :LANES] * rs * gs[l : l + 1, cols]
                rows = lax.broadcasted_iota(jnp.int32, g.shape, 0)
                prev = jnp.where(rows == 0, 0.0, pltpu.roll(g, 1, 0))
                nxt = jnp.where(rows == n_tok - 1, 0.0, pltpu.roll(g, n_tok - 1, 0))
                mixed = taps[l, 0:1, cols] * prev + taps[l, 1:2, cols] * g + taps[l, 2:3, cols] * nxt
                part[j, :, 0:LANES] = mixed.astype(bf16)
                part[j, :, LANES : 2 * LANES] = (acc[:, LANES:] * rs * us[l : l + 1, cols]).astype(bf16)
                for ch in range(CHUNKS):
                    core_copy(ch, j).start()

            @pl.when(j >= LAG)
            def _():
                x_step(0, j - LAG)

            return carry

        lax.fori_loop(0, tiles + LAG, gate_step, 0)

        load(l, 2).wait()

        def cast_step(i, carry):
            r = pl.ds(pl.multiple_of(i * LANES, LANES), LANES)
            dwb[r, :] = dw[l, r, :].astype(bf16)
            return carry

        lax.fori_loop(0, tiles, cast_step, 0)

        def h_copy(ch, j, n):
            cols = pl.ds(pl.multiple_of(j * LANES, LANES), LANES)
            block = hid.at[l, block_rows(ch, c, 1 - x if n == 2 else x), cols]
            return remote(
                block, block, (hsem.at[0, l, ch, n, j], hsem.at[1, l, ch, n, j]), x_dev if n == 0 else core_dev
            )

        def hidden(ch):
            my_rows = block_rows(ch, c, x)

            def step(j, carry):
                cols = pl.ds(pl.multiple_of(j * LANES, LANES), LANES)
                x_copy(ch, j).wait_recv()
                s = (
                    part[j, my_rows, :].astype(f32)
                    + crecv[l, ch, j, m_local, :].astype(f32)
                    + xrecv[l, ch, j].astype(f32)
                )
                mixed = s[:, :LANES] + bias[l : l + 1, cols]
                hid[l, my_rows, cols] = (mixed / (1.0 + jnp.exp(-mixed)) * s[:, LANES:]).astype(bf16)
                h_copy(ch, j, 0).start()
                h_copy(ch, j, 1).start()
                return carry

            lax.fori_loop(0, tiles, step, 0)

        def gather_hidden(ch):
            def forward_step(j, carry):
                h_copy(ch, j, 0).wait_recv()
                h_copy(ch, j, 2).start()
                return carry

            lax.fori_loop(0, tiles, forward_step, 0)

            def gathered_step(j, carry):
                h_copy(ch, j, 1).wait_recv()
                h_copy(ch, j, 2).wait_recv()
                return carry

            lax.fori_loop(0, tiles, gathered_step, 0)

        def y_copy(ch, k):
            zz = lax.rem(z + k, n_z)
            return remote(
                ysend.at[ch, zr(zz), :],
                yrecv.at[l, ch, zr(zz), :],
                (ysem.at[0, l, ch, k - 1], ysem.at[1, l, ch, k - 1]),
                y_dev,
            )

        def down(ch):
            width = 256
            other_y = pl.ds(pl.multiple_of(ch * span + (1 - y) * half, half), half)
            own_y = pl.ds(pl.multiple_of(ch * span + y * half, half), half)

            def down_other(i, carry):
                cols = pl.ds(pl.multiple_of(i * width, width), width)
                ysend[ch, :, cols] = jnp.dot(
                    hid[l, other_y, :], dwb[:, cols], preferred_element_type=f32
                ).astype(bf16)
                return carry

            def down_own(i, carry):
                cols = pl.ds(pl.multiple_of(i * width, width), width)
                own[ch, :, cols] = jnp.dot(hid[l, own_y, :], dwb[:, cols], preferred_element_type=f32)
                return carry

            lax.fori_loop(0, d_loc // width, down_other, 0)
            for k in range(1, n_z + 1):
                y_copy(ch, k).start()
            lax.fori_loop(0, d_loc // width, down_own, 0)

        def z_copy(ch, k):
            zz = lax.rem(z + k, n_z)
            return remote(
                zsend.at[ch, zr(zz), :],
                zrecv.at[l, ch, k - 1],
                (zsem.at[0, l, ch, k - 1], zsem.at[1, l, ch, k - 1]),
                z_dev(k),
            )

        def spread_z(ch):
            for k in range(1, n_z):
                zz = lax.rem(z + k, n_z)
                y_copy(ch, k).wait_recv()
                zsend[ch, zr(zz), :] = (own[ch, zr(zz), :] + yrecv[l, ch, zr(zz), :].astype(f32)).astype(bf16)
                z_copy(ch, k).start()

        def gather_z(ch, k):
            block = hnew.at[l, hr(ch, y, z), :]
            return remote(block, block, (asem.at[0, l, ch, k - 1], asem.at[1, l, ch, k - 1]), z_dev(k))

        def gather_y(ch, k):
            block = hnew.at[l, hr(ch, y, lax.rem(z + n_z - k, n_z)), :]
            return remote(block, block, (fsem.at[0, l, ch, k], fsem.at[1, l, ch, k]), y_dev)

        def finish(ch):
            y_copy(ch, n_z).wait_recv()
            acc = own[ch, zr(z), :] + yrecv[l, ch, zr(z), :].astype(f32)
            for k in range(1, n_z):
                z_copy(ch, k).wait_recv()
                acc = acc + zrecv[l, ch, k - 1].astype(f32)
            mine = hr(ch, y, z)
            new = residual_scale * h[mine, :].astype(f32) + acc * ds_[l : l + 1, :]
            hnew[l, mine, :] = new.astype(bf16)
            for k in range(1, n_z):
                gather_z(ch, k).start()
            gather_y(ch, 0).start()

        def forward(ch):
            for k in range(1, n_z):
                gather_z(ch, k).wait_recv()
                gather_y(ch, k).start()

        def second_x(i, carry):
            x_step(1, i)
            return carry

        hidden(0)
        lax.fori_loop(0, tiles, second_x, 0)
        gather_hidden(0)
        down(0)
        spread_z(0)
        hidden(1)
        finish(0)
        gather_hidden(1)
        down(1)
        forward(0)
        spread_z(1)
        finish(1)
        forward(1)
        for ch in range(CHUNKS):
            for k in range(n_z):
                gather_y(ch, k).wait_recv()

        for ch in range(CHUNKS):

            def sent_step(j, carry, ch=ch):
                core_copy(ch, j).wait_send()
                x_copy(ch, j).wait_send()
                for n in range(3):
                    h_copy(ch, j, n).wait_send()
                return carry

            lax.fori_loop(0, tiles, sent_step, 0)
            for k in range(1, n_z + 1):
                y_copy(ch, k).wait_send()
            for k in range(1, n_z):
                z_copy(ch, k).wait_send()
                gather_z(ch, k).wait_send()
            for k in range(n_z):
                gather_y(ch, k).wait_send()
    out[...] = hnew[layers - 1]


def fused(n_ra, tokens, gate_weight, up_weight, down_weight, gate_scale, up_scale, down_scale, gain, taps, bias, d_all):
    n_tok, d_loc = tokens.shape
    layers, _, f_loc = gate_weight.shape
    n_z = n_ra // 2
    tiles = f_loc // LANES
    half, quarter = n_tok // CHUNKS // 2, n_tok // CHUNKS // 4
    f32, bf16 = jnp.float32, jnp.bfloat16
    dma = pltpu.SemaphoreType.DMA
    vmem, hbm = pl.BlockSpec(memory_space=pltpu.VMEM), pl.BlockSpec(memory_space=pl.ANY)
    zrows = half // n_z
    return pl.pallas_call(
        functools.partial(kernel, (layers, n_tok, d_loc, f_loc, d_all, n_z)),
        out_shape=jax.ShapeDtypeStruct((n_tok, d_loc), bf16),
        in_specs=[vmem, hbm, hbm, hbm] + [vmem] * 6,
        out_specs=vmem,
        scratch_shapes=[
            pltpu.VMEM((layers, d_loc, f_loc), f32),
            pltpu.VMEM((layers, d_loc, f_loc), f32),
            pltpu.VMEM((layers, f_loc, d_loc), f32),
            pltpu.VMEM((f_loc, d_loc), bf16),
            pltpu.VMEM((n_tok, d_loc), bf16),
            pltpu.VMEM((n_tok, LANES), f32),
            pltpu.VMEM((layers, 4, 8, LANES), f32),
            pltpu.VMEM((tiles, n_tok, 2 * LANES), bf16),
            pltpu.VMEM((layers, CHUNKS, tiles, half, 2 * LANES), bf16),
            pltpu.VMEM((CHUNKS, tiles, quarter, 2 * LANES), bf16),
            pltpu.VMEM((layers, CHUNKS, tiles, quarter, 2 * LANES), bf16),
            pltpu.VMEM((layers, n_tok, f_loc), bf16),
            pltpu.VMEM((CHUNKS, half, d_loc), bf16),
            pltpu.VMEM((CHUNKS, half, d_loc), f32),
            pltpu.VMEM((layers, CHUNKS, half, d_loc), bf16),
            pltpu.VMEM((CHUNKS, half, d_loc), bf16),
            pltpu.VMEM((layers, CHUNKS, n_z - 1, zrows, d_loc), bf16),
            pltpu.VMEM((layers, n_tok, d_loc), bf16),
            dma((layers, 3)),
            dma((2, layers, 3)),
            dma((2, layers, CHUNKS, tiles)),
            dma((2, layers, CHUNKS, tiles)),
            dma((2, layers, CHUNKS, 3, tiles)),
            dma((2, layers, CHUNKS, n_z)),
            dma((2, layers, CHUNKS, n_z - 1)),
            dma((2, layers, CHUNKS, n_z - 1)),
            dma((2, layers, CHUNKS, n_z)),
        ],
        compiler_params=pltpu.CompilerParams(
            collective_id=0, has_side_effects=True, vmem_limit_bytes=67_043_328
        ),
    )(tokens, gate_weight, up_weight, down_weight, gate_scale, up_scale, down_scale, gain, taps, bias)


def plain(tokens, gate_weight, up_weight, down_weight, gate_scale, up_scale, down_scale, gain, conv_taps, bias, d_all):
    hstate = tokens
    for layer in range(gate_weight.shape[0]):
        wide = hstate.astype(jnp.float32)
        squares = jnp.sum(wide * wide, axis=1)
        operand = (wide * gain[layer]).astype(jnp.bfloat16)
        gate_part = jnp.dot(operand, gate_weight[layer].astype(jnp.bfloat16), preferred_element_type=jnp.float32)
        up_part = jnp.dot(operand, up_weight[layer].astype(jnp.bfloat16), preferred_element_type=jnp.float32)
        gate_sum, up_sum, square_sum = lax.psum((gate_part, up_part, squares), "cb")
        rscale = lax.rsqrt(square_sum / d_all + norm_eps)[:, None]
        gate = gate_sum * rscale * gate_scale[layer]
        upward = up_sum * rscale * up_scale[layer]
        padded = jnp.pad(gate, ((1, 1), (0, 0)))
        taps = conv_taps[layer]
        mixed = taps[0] * padded[:-2] + taps[1] * padded[1:-1] + taps[2] * padded[2:] + bias[layer]
        hidden = (jax.nn.silu(mixed) * upward).astype(jnp.bfloat16)
        term = jnp.dot(hidden, down_weight[layer].astype(jnp.bfloat16), preferred_element_type=jnp.float32)
        branch = lax.psum(term, "ra") * down_scale[layer]
        hstate = (residual_scale * wide + branch).astype(jnp.bfloat16)
    return hstate


def solution(mesh):
    n_ra, n_cb = mesh.shape["ra"], mesh.shape["cb"]

    def per_device(*args):
        n_tok, d_loc = args[0].shape
        f_loc = args[1].shape[2]
        fits = n_cb == 4 and n_ra % 2 == 0 and n_ra >= 4 and n_tok % (16 * CHUNKS * n_ra) == 0 and n_tok <= 8 * LANES
        fits = fits and f_loc % LANES == 0 and d_loc % 256 == 0 and f_loc > LAG * LANES
        if fits:
            return fused(n_ra, *args, d_loc * n_cb)
        return plain(*args, d_loc * n_cb)

    in_specs = (
        P(None, "cb"),
        P(None, "cb", "ra"),
        P(None, "cb", "ra"),
        P(None, "ra", "cb"),
        P(None, "ra"),
        P(None, "ra"),
        P(None, "cb"),
        P(None, "cb"),
        P(None, None, "ra"),
        P(None, "ra"),
    )
    return jax.shard_map(
        per_device, mesh=mesh, in_specs=in_specs, out_specs=P(None, "cb"), check_vma=False
    )
```

profile of v0, /device:TPU:0, one launch (start us, length us, event | category | flops | bytes accessed | tf_op | source)
XLA Modules:
  0.0 133.3 jit_solution(3809554125032544110)
XLA Ops:
  0.0 1.4 %copy.11.taps = f32[2,3,1408]{2,1,0:T(4,128)} copy(f32[2,3,1408]{2,0,1:T(2,128)} %param.18) | data formatting | bytes 67584 | tf_op args[8]
  1.4 129.7 %shard_map.100 = bf16[512,1024]{1,0:T(8,128)(2,1)} custom-call(bf16[512,1024]{1,0:T(8,128)(2,1)} %tok.1, f32[2,1024,1408]{2,1,0:T(8,128)} %gw_hbm.1, f32[2,1024,1408]{2,1,0:T(8,128)} %uw_hbm.1, f32[2,1408,1024]{2,1,0:T(8,128)} %dw_hbm.1, f32[2,1408]{1,0:T(2,128)} %gs.1, f32[2,1408]{1,0:T(2,128)} %us.1, f32[2,1024]{1,0:T(2,128)} %ds_.1, f32[2,1024]{1,0:T(2,128)} %gain.1, ...), custom_call_target="tpu_custom_call" | custom-call | tf_op jit(solution)/shard_map/pallas_call | solution.py:353
  131.1 2.3 %copy.13 = bf16[512,1024]{1,0:T(8,128)(2,1)} copy(bf16[512,1024]{1,0:T(8,128)(2,1)} %shard_map.100) | data formatting | bytes 2097152
where the time goes:
time: 134 us; the launch traced here: 133 us
  Pallas kernels  130 us (97%)
  local copies, waits for them, and re-layouts  3.65 us (3%)
    pallas_call x1, Pallas kernels, fused(): pl.pallas_call(functools.partial(kernel, (layers, n_tok, d_loc, f_loc, d_...  130 us
    unnamed x2, local copies, waits for them, and re-layouts  3.65 us

commit v1 on v0

v1 whole, which is shorter than its diff:
```python
import functools

import jax
import jax.numpy as jnp
from jax import lax
from jax.experimental import pallas as pl
from jax.experimental.pallas import tpu as pltpu
from jax.sharding import PartitionSpec as P

MESH = pl.DeviceIdType.MESH
norm_eps = 1e-06
residual_scale = 0.25
LANES = 128
PACK = 16
CHUNKS = 4
LAG = 2
STAGES = "GABHIFJDZEWNR"


def row_chunks(n_tok, layers):
    step, shift = n_tok // CHUNKS, 4 * PACK
    chunks = []
    for l in range(layers):
        ends = [e - l * shift for e in range(step, n_tok + 1, step)]
        ends = [e for e in ends if 0 < e < n_tok] + [n_tok]
        chunks.append(list(zip([0] + ends[:-1], ends)))
    return chunks


def plan(chunks):
    n_tok, layers = chunks[0][-1][1], len(chunks)
    near, side, far = 1.0, 2.1, 2.9
    link = {"x": 0.0, "y": 0.0, "z": 0.0}
    cost = {
        "G": (1.0, 1.4), "A": (0.1, 0.15), "B": (0.1, 0.15), "H": (0.1, 0.2), "I": (0.1, 0.2), "F": (0.1, 0.0),
        "J": (0.1, 0.0), "D": (0.35, 0.65), "Z": (0.1, 0.1), "E": (0.1, 0.1), "W": (0.1, 0.0), "N": (0.1, 0.25),
        "R": (0.2, 0.1),
    }
    done, arrive, order, now = {}, {}, [], 0.0
    todo = [(l, k, s) for l in range(layers) for k in range(len(chunks[l])) for s in STAGES]
    todo = [o for o in todo if not (o[0] == layers - 1 and o[2] == "R")]

    def send(name, start, length, delay):
        begin = max(link[name], start)
        link[name] = begin + length
        return begin + length + delay

    def ready(l, k, s):
        needs = []
        if s == "G":
            if k > 0:
                needs.append((l, k - 1, "G"))
            if l > 0:
                last = min(chunks[l][k][1] + PACK, n_tok)
                needs += [(l - 1, j, "R") for j, (a, _) in enumerate(chunks[l - 1]) if a < last]
        else:
            needs.append((l, k, STAGES[STAGES.index(s) - 1]))
            if s == "A" and k > 0:
                needs.append((l, k - 1, "B"))
            if s == "B" and k > 0:
                needs.append((l, k - 1, "I"))
            if s == "N" and k + 1 < len(chunks[l]):
                needs.append((l, k + 1, "G"))
        if any(o not in done for o in needs):
            return None
        return max([0.0] + [done[o] for o in needs] + [arrive.get((l, k, s), 0.0)])

    while todo:
        best = None
        for o in todo:
            at = ready(*o)
            if at is not None:
                rank = (round(max(now, at), 1), o[0], o[1], STAGES.index(o[2]))
                if best is None or rank < best[0]:
                    best = (rank, o, max(now, at))
        _, o, start = best
        l, k, s = o
        q = (chunks[l][k][1] - chunks[l][k][0]) / 128
        now = start + cost[s][0] + cost[s][1] * q
        done[o] = now
        todo.remove(o)
        order.append(o)
        if s == "G":
            arrive[l, k, "A"] = now + near
        if s == "A":
            arrive[l, k, "H"] = send("x", start, 1.93 * q, side)
        if s == "B":
            arrive[l, k, "I"] = send("x", start, 1.93 * q, side)
        if s == "H":
            arrive[l, k, "F"] = send("x", start, 0.97 * q, side)
        if s == "I":
            arrive[l, k, "J"] = send("x", start, 0.97 * q, side)
        if s == "J":
            arrive[l, k, "D"] = now + near
        if s == "D":
            arrive[l, k, "E"] = send("y", now, 2.8 * q, side)
            arrive[l, k, "Z"] = arrive[l, k, "E"] - 2.1 * q
        if s == "Z":
            arrive[l, k, "E"] = max(send("z", start, 2.8 * q, far), arrive[l, k, "E"] + far)
        if s == "E":
            arrive[l, k, "N"] = send("z", now, 2.8 * q, far)
            arrive[l, k, "W"] = arrive[l, k, "N"] - 1.4 * q
        if s == "W":
            arrive[l, k, "N"] = max(send("y", start, 2.8 * q, side), arrive[l, k, "N"] + side)
        if s == "N":
            arrive[l, k, "R"] = now + side
    return order, now


def kernel(
    sizes,
    tok,
    gw_hbm,
    uw_hbm,
    dw_hbm,
    gs,
    us,
    ds_,
    gain,
    taps,
    bias,
    out,
    gw,
    uw,
    dw,
    dwb,
    operand,
    rsb,
    stat,
    part,
    crecv,
    xsend,
    xrecv,
    hid,
    ysend,
    own,
    yrecv,
    zsend,
    zrecv,
    hnew,
    wsem,
    lsem,
    ssem,
    csem,
    xsem,
    hsem,
    ysem,
    zsem,
    asem,
    fsem,
):
    chunks, n_tok, d_loc, f_loc, d_all, n_z = sizes
    layers = len(chunks)
    tiles = f_loc // LANES
    units = (tiles + 1) // 2
    pairs = tiles // 2
    piece, d_half = d_loc // (2 * n_z), d_loc // 2
    first = [sum(len(c) for c in chunks[:l]) for l in range(layers)]
    f32, bf16 = jnp.float32, jnp.bfloat16
    ra, cb = lax.axis_index("ra"), lax.axis_index("cb")
    z, y = ra // 2, ra % 2
    x, c = cb // 2, cb % 2
    core_dev = (ra, x * 2 + (1 - c))
    x_dev = (ra, (1 - x) * 2 + c)
    y_dev = (z * 2 + (1 - y), cb)

    def z_dev(i):
        return (lax.rem(z + i, n_z) * 2 + y, cb)

    def remote(src, dst, sems, dev):
        return pltpu.make_async_remote_copy(
            src_ref=src, dst_ref=dst, send_sem=sems[0], recv_sem=sems[1], device_id=dev, device_id_type=MESH
        )

    def span_of(at, width, size=1):
        return pl.ds(pl.multiple_of(at * width, width), size * width)

    def each(fn, begin=0, end=units):
        stop = min(end, pairs)
        if stop > begin:

            def step(u, carry):
                fn(u, 2)
                return carry

            lax.fori_loop(begin, stop, step, 0)
        if end > pairs:
            fn(pairs, 1)

    def first_load(u, w, n):
        src, dst = ((gw_hbm, gw), (uw_hbm, uw))[n]
        cols = span_of(u * 2, LANES, w)
        return pltpu.make_async_copy(src.at[0, :, cols], dst.at[0, :, cols], wsem.at[u, n])

    def load(l, n):
        src, dst = ((gw_hbm, gw), (uw_hbm, uw), (dw_hbm, dw))[n]
        return pltpu.make_async_copy(src.at[l], dst if n == 2 else dst.at[l], lsem.at[l, n])

    def start_first(u, w):
        first_load(u, w, 0).start()
        first_load(u, w, 1).start()

    each(start_first)

    barrier = pltpu.get_barrier_semaphore()
    peers = [(ra, lax.rem(cb + k, 4)) for k in range(1, 4)] + [y_dev] + [z_dev(k) for k in range(1, n_z)]
    for dev in peers:
        pl.semaphore_signal(barrier, inc=1, device_id=dev, device_id_type=MESH)
    pl.semaphore_wait(barrier, len(peers))

    def stat_copy(n, k):
        return remote(stat.at[n, 0], stat.at[n, k], (ssem.at[0, n, k - 1], ssem.at[1, n, k - 1]), (ra, lax.rem(cb + k, 4)))

    def picked(s, e):
        lane = lax.broadcasted_iota(jnp.int32, (e - s, LANES), 1)
        row = lax.broadcasted_iota(jnp.int32, (e - s, LANES), 0)
        return lane == lax.shift_right_logical(row + s, 3)

    def squares(n, h, l, s, e):
        wide = h[s:e, :].astype(f32)
        ssq = jnp.sum(wide * wide, axis=1, keepdims=True)
        packed = jnp.where(picked(s, e), jnp.broadcast_to(ssq, (e - s, LANES)), 0.0)
        stat[n, 0] = jnp.sum(packed.reshape((e - s) // 8, 8, LANES), axis=0)
        for k in range(1, 4):
            stat_copy(n, k).start()
        operand[s:e, :] = (wide * gain[l : l + 1, :]).astype(bf16)

    def scale_rows(n, s, e):
        for k in range(1, 4):
            stat_copy(n, k).wait()
        total = stat[n, 0] + stat[n, 1] + stat[n, 2] + stat[n, 3]
        spread = jnp.broadcast_to(total[None], ((e - s) // 8, 8, LANES)).reshape(e - s, LANES)
        summed = jnp.sum(jnp.where(picked(s, e), spread, 0.0), axis=1, keepdims=True)
        rsb[s:e, :] = jnp.broadcast_to(lax.rsqrt(summed / d_all + norm_eps), (e - s, LANES))

    def steps_of(l, k):
        s, e = chunks[l][k]
        at = first[l] + k
        half, quarter = (e - s) // 2, (e - s) // 4
        lo, hi = max(s - PACK, 0), min(e + PACK, n_tok)
        h = tok if l == 0 else hnew.at[l - 1]

        def block_rows(cc, xx):
            return pl.ds(pl.multiple_of(s + cc * half + xx * quarter, PACK), quarter)

        def local_rows(xx):
            return pl.ds(pl.multiple_of(s // 2 + xx * quarter, PACK), quarter)

        x_rows = slice(s // 4, e // 4)

        def core_copy(u, w):
            rows = pl.ds(pl.multiple_of(s + (1 - c) * half, PACK), half)
            cols = span_of(u * 4, LANES, 2 * w)
            dst = crecv.at[l, s // 2 : e // 2, cols]
            return remote(part.at[rows, cols], dst, (csem.at[0, at, u], csem.at[1, at, u]), core_dev)

        def x_copy(u, w):
            cols = span_of(u * 4, LANES, 2 * w)
            sems = (xsem.at[0, at, u], xsem.at[1, at, u])
            return remote(xsend.at[x_rows, cols], xrecv.at[l, x_rows, cols], sems, x_dev)

        def h_copy(u, w, n):
            cols = span_of(u * 2, LANES, w)
            block = hid.at[l, block_rows(c, 1 - x if n == 2 else x), cols]
            return remote(block, block, (hsem.at[0, at, n, u], hsem.at[1, at, n, u]), x_dev if n == 0 else core_dev)

        def y_copy(i):
            cols = span_of(lax.rem(z + i, n_z), piece)
            sems = (ysem.at[0, at, i - 1], ysem.at[1, at, i - 1])
            return remote(ysend.at[s:e, cols], yrecv.at[l, s:e, cols], sems, y_dev)

        def z_copy(i):
            cols = span_of(lax.rem(z + i, n_z), piece)
            sems = (zsem.at[0, at, i - 1], zsem.at[1, at, i - 1])
            return remote(zsend.at[s:e, cols], zrecv.at[l, i - 1, s:e, :], sems, z_dev(i))

        def gather_z(i):
            block = hnew.at[l, s:e, span_of(y * n_z + z, piece)]
            return remote(block, block, (asem.at[0, at, i - 1], asem.at[1, at, i - 1]), z_dev(i))

        def gather_y(i):
            block = hnew.at[l, s:e, span_of(y * n_z + lax.rem(z + n_z - i, n_z), piece)]
            return remote(block, block, (fsem.at[0, at, i], fsem.at[1, at, i]), y_dev)

        def gate_unit(u, w):
            if l == 0 and k == 0:
                first_load(u, w, 0).wait()
                first_load(u, w, 1).wait()
            cols = span_of(u * 2, LANES, w)
            weights = jnp.concatenate([gw[l, :, cols].astype(bf16), uw[l, :, cols].astype(bf16)], axis=1)
            acc = jnp.dot(operand[lo:hi, :], weights, preferred_element_type=f32)
            rs = rsb[lo:hi, :]
            rows = lax.broadcasted_iota(jnp.int32, rs.shape, 0)
            for i in range(w):
                col = span_of(u * 2 + i, LANES)
                g = acc[:, i * LANES : (i + 1) * LANES] * rs * gs[l : l + 1, col]
                prev, nxt = pltpu.roll(g, 1, 0), pltpu.roll(g, hi - lo - 1, 0)
                if s == 0:
                    prev = jnp.where(rows == 0, 0.0, prev)
                if e == n_tok:
                    nxt = jnp.where(rows == hi - lo - 1, 0.0, nxt)
                mixed = taps[l, 0:1, col] * prev + taps[l, 1:2, col] * g + taps[l, 2:3, col] * nxt
                upward = acc[:, (w + i) * LANES : (w + i + 1) * LANES] * rs * us[l : l + 1, col]
                part[s:e, span_of(u * 4 + 2 * i, LANES)] = mixed[s - lo : e - lo].astype(bf16)
                part[s:e, span_of(u * 4 + 2 * i + 1, LANES)] = upward[s - lo : e - lo].astype(bf16)
            core_copy(u, w).start()

        def x_unit(u, w):
            core_copy(u, w).wait_recv()
            cols = span_of(u * 4, LANES, 2 * w)
            mine = part[block_rows(c, 1 - x), cols].astype(f32)
            xsend[x_rows, cols] = (mine + crecv[l, local_rows(1 - x), cols].astype(f32)).astype(bf16)
            x_copy(u, w).start()

        def hidden_unit(u, w):
            x_copy(u, w).wait_recv()
            cols = span_of(u * 4, LANES, 2 * w)
            rows = block_rows(c, x)
            total = (
                part[rows, cols].astype(f32)
                + crecv[l, local_rows(x), cols].astype(f32)
                + xrecv[l, x_rows, cols].astype(f32)
            )
            for i in range(w):
                col = span_of(u * 2 + i, LANES)
                mixed = total[:, 2 * i * LANES : (2 * i + 1) * LANES] + bias[l : l + 1, col]
                upward = total[:, (2 * i + 1) * LANES : (2 * i + 2) * LANES]
                hid[l, rows, col] = (mixed / (1.0 + jnp.exp(-mixed)) * upward).astype(bf16)
            h_copy(u, w, 0).start()
            h_copy(u, w, 1).start()

        def forward_unit(u, w):
            h_copy(u, w, 0).wait_recv()
            h_copy(u, w, 2).start()

        def gathered_unit(u, w):
            h_copy(u, w, 1).wait_recv()
            h_copy(u, w, 2).wait_recv()

        middle = units // 2

        def gate():
            each(gate_unit)

        def gate_first():
            def step(u, carry):
                gate_unit(u, 2)

                @pl.when(u >= LAG)
                def _():
                    x_unit(u - LAG, 2)

                return carry

            lax.fori_loop(0, pairs, step, 0)
            if units > pairs:
                gate_unit(pairs, 1)
            each(x_unit, max(pairs - LAG, 0))

        def down():
            each(gathered_unit)
            rows = hid[l, s:e, :]
            other = jnp.dot(rows, dwb[l, :, span_of(1 - y, d_half)], preferred_element_type=f32)
            ysend[s:e, :] = other.astype(bf16)
            for i in range(1, n_z + 1):
                y_copy(i).start()
            own[s:e, :] = jnp.dot(rows, dwb[l, :, span_of(y, d_half)], preferred_element_type=f32)

        def spread():
            for i in range(1, n_z):
                cols = span_of(lax.rem(z + i, n_z), piece)
                y_copy(i).wait_recv()
                zsend[s:e, cols] = (own[s:e, cols] + yrecv[l, s:e, cols].astype(f32)).astype(bf16)
                z_copy(i).start()

        def finish():
            cols, mine = span_of(z, piece), span_of(y * n_z + z, piece)
            y_copy(n_z).wait_recv()
            acc = own[s:e, cols] + yrecv[l, s:e, cols].astype(f32)
            for i in range(1, n_z):
                z_copy(i).wait_recv()
                acc = acc + zrecv[l, i - 1, s:e, :].astype(f32)
            new = residual_scale * h[s:e, mine].astype(f32) + acc * ds_[l : l + 1, mine]
            hnew[l, s:e, mine] = new.astype(bf16)
            for i in range(1, n_z):
                gather_z(i).start()
            gather_y(0).start()

        def forward():
            for i in range(1, n_z):
                gather_z(i).wait_recv()
                gather_y(i).start()

        def sent_unit(u, w):
            core_copy(u, w).wait_send()
            x_copy(u, w).wait_send()
            for n in range(3):
                h_copy(u, w, n).wait_send()

        def arrived():
            for i in range(n_z):
                gather_y(i).wait_recv()
            if l + 1 < layers:
                squares(1 + at, hnew.at[l], l + 1, s, e)
            else:
                out[s:e, :] = hnew[l, s:e, :]
            each(sent_unit)
            for i in range(1, n_z + 1):
                y_copy(i).wait_send()
            for i in range(1, n_z):
                z_copy(i).wait_send()

        def sent():
            for i in range(1, n_z):
                gather_z(i).wait_send()
            for i in range(n_z):
                gather_y(i).wait_send()

        return {
            "G": gate_first if k == 0 else gate,
            "A": functools.partial(each, x_unit, 0, middle),
            "B": functools.partial(each, x_unit, middle),
            "H": functools.partial(each, hidden_unit, 0, middle),
            "I": functools.partial(each, hidden_unit, middle),
            "F": functools.partial(each, forward_unit, 0, middle),
            "J": functools.partial(each, forward_unit, middle),
            "D": down,
            "Z": spread,
            "E": finish,
            "W": forward,
            "N": arrived,
            "R": functools.partial(scale_rows, 1 + at, s, e),
            "sent": sent,
        }

    def cast_down(l):
        load(l, 2).wait()

        def step(i, carry):
            r = span_of(i, LANES)
            dwb[l, r, :] = dw[r, :].astype(bf16)
            return carry

        lax.fori_loop(0, tiles, step, 0)
        if l + 1 < layers:
            load(l + 1, 2).start()

    squares(0, tok, 0, 0, n_tok)
    scale_rows(0, 0, n_tok)
    steps = {(l, k): steps_of(l, k) for l in range(layers) for k in range(len(chunks[l]))}
    for l, k, s in plan(chunks)[0]:
        if s == "G" and l > 0 and k == 0:
            load(l, 0).wait()
            load(l, 1).wait()
        if s == "H" and (l, k) == (0, 0):
            cast_down(0)
        if s == "E" and k == 0 and l + 1 < layers:
            cast_down(l + 1)
        if k == 0 and s in "AB":
            continue
        steps[l, k][s]()
        if s == "G" and (l, k) == (0, 0):
            load(0, 2).start()
            for ll in range(1, layers):
                load(ll, 0).start()
                load(ll, 1).start()
    for group in steps.values():
        group["sent"]()


def fused(n_ra, tokens, gate_weight, up_weight, down_weight, gate_scale, up_scale, down_scale, gain, taps, bias, d_all):
    n_tok, d_loc = tokens.shape
    layers, _, f_loc = gate_weight.shape
    n_z = n_ra // 2
    chunks = row_chunks(n_tok, layers)
    total = sum(len(c) for c in chunks)
    tiles = f_loc // LANES
    units = (tiles + 1) // 2
    f32, bf16 = jnp.float32, jnp.bfloat16
    dma = pltpu.SemaphoreType.DMA
    vmem, hbm = pl.BlockSpec(memory_space=pltpu.VMEM), pl.BlockSpec(memory_space=pl.ANY)
    return pl.pallas_call(
        functools.partial(kernel, (chunks, n_tok, d_loc, f_loc, d_all, n_z)),
        out_shape=jax.ShapeDtypeStruct((n_tok, d_loc), bf16),
        in_specs=[vmem, hbm, hbm, hbm] + [vmem] * 6,
        out_specs=vmem,
        scratch_shapes=[
            pltpu.VMEM((layers, d_loc, f_loc), f32),
            pltpu.VMEM((layers, d_loc, f_loc), f32),
            pltpu.VMEM((f_loc, d_loc), f32),
            pltpu.VMEM((layers, f_loc, d_loc), bf16),
            pltpu.VMEM((n_tok, d_loc), bf16),
            pltpu.VMEM((n_tok, LANES), f32),
            pltpu.VMEM((1 + total, 4, 8, LANES), f32),
            pltpu.VMEM((n_tok, 2 * f_loc), bf16),
            pltpu.VMEM((layers, n_tok // 2, 2 * f_loc), bf16),
            pltpu.VMEM((n_tok // 4, 2 * f_loc), bf16),
            pltpu.VMEM((layers, n_tok // 4, 2 * f_loc), bf16),
            pltpu.VMEM((layers, n_tok, f_loc), bf16),
            pltpu.VMEM((n_tok, d_loc // 2), bf16),
            pltpu.VMEM((n_tok, d_loc // 2), f32),
            pltpu.VMEM((layers, n_tok, d_loc // 2), bf16),
            pltpu.VMEM((n_tok, d_loc // 2), bf16),
            pltpu.VMEM((layers, n_z - 1, n_tok, d_loc // n_ra), bf16),
            pltpu.VMEM((layers, n_tok, d_loc), bf16),
            dma((units, 2)),
            dma((layers, 3)),
            dma((2, 1 + total, 3)),
            dma((2, total, units)),
            dma((2, total, units)),
            dma((2, total, 3, units)),
            dma((2, total, n_z)),
            dma((2, total, n_z - 1)),
            dma((2, total, n_z - 1)),
            dma((2, total, n_z)),
        ],
        compiler_params=pltpu.CompilerParams(
            collective_id=0, has_side_effects=True, vmem_limit_bytes=67_043_328
        ),
    )(tokens, gate_weight, up_weight, down_weight, gate_scale, up_scale, down_scale, gain, taps, bias)


def plain(tokens, gate_weight, up_weight, down_weight, gate_scale, up_scale, down_scale, gain, conv_taps, bias, d_all):
    hstate = tokens
    for layer in range(gate_weight.shape[0]):
        wide = hstate.astype(jnp.float32)
        squares = jnp.sum(wide * wide, axis=1)
        operand = (wide * gain[layer]).astype(jnp.bfloat16)
        gate_part = jnp.dot(operand, gate_weight[layer].astype(jnp.bfloat16), preferred_element_type=jnp.float32)
        up_part = jnp.dot(operand, up_weight[layer].astype(jnp.bfloat16), preferred_element_type=jnp.float32)
        gate_sum, up_sum, square_sum = lax.psum((gate_part, up_part, squares), "cb")
        rscale = lax.rsqrt(square_sum / d_all + norm_eps)[:, None]
        gate = gate_sum * rscale * gate_scale[layer]
        upward = up_sum * rscale * up_scale[layer]
        padded = jnp.pad(gate, ((1, 1), (0, 0)))
        taps = conv_taps[layer]
        mixed = taps[0] * padded[:-2] + taps[1] * padded[1:-1] + taps[2] * padded[2:] + bias[layer]
        hidden = (jax.nn.silu(mixed) * upward).astype(jnp.bfloat16)
        term = jnp.dot(hidden, down_weight[layer].astype(jnp.bfloat16), preferred_element_type=jnp.float32)
        branch = lax.psum(term, "ra") * down_scale[layer]
        hstate = (residual_scale * wide + branch).astype(jnp.bfloat16)
    return hstate


def solution(mesh):
    n_ra, n_cb = mesh.shape["ra"], mesh.shape["cb"]

    def per_device(*args):
        n_tok, d_loc = args[0].shape
        f_loc = args[1].shape[2]
        fits = n_cb == 4 and n_ra % 2 == 0 and n_ra >= 4 and n_tok % (4 * PACK * CHUNKS) == 0 and n_tok <= 8 * LANES
        fits = fits and f_loc % LANES == 0 and d_loc % (LANES * n_ra) == 0 and f_loc >= 2 * LAG * LANES
        if fits:
            return fused(n_ra, *args, d_loc * n_cb)
        return plain(*args, d_loc * n_cb)

    in_specs = (
        P(None, "cb"),
        P(None, "cb", "ra"),
        P(None, "cb", "ra"),
        P(None, "ra", "cb"),
        P(None, "ra"),
        P(None, "ra"),
        P(None, "cb"),
        P(None, "cb"),
        P(None, None, "ra"),
        P(None, "ra"),
    )
    return jax.shard_map(
        per_device, mesh=mesh, in_specs=in_specs, out_specs=P(None, "cb"), check_vma=False
    )
```

time: 134 us -> 117 us (0.87)
  Pallas kernels: 130 us -> 113 us
    pallas_call x1, Pallas kernels: 130 us -> 113 us  [fused(): pl.pallas_call(functools.partial(kernel, (chunks, n_tok, d_loc, f_loc, d_...]
where the time goes in v1:
time: 117 us
  Pallas kernels  113 us (97%)
  local copies, waits for them, and re-layouts  3.65 us (3%)
    pallas_call x1, Pallas kernels, fused(): pl.pallas_call(functools.partial(kernel, (chunks, n_tok, d_loc, f_loc, d_...  113 us
    unnamed x2, local copies, waits for them, and re-layouts  3.65 us

profile of v1, /device:TPU:0, one launch (start us, length us, event | category | flops | bytes accessed | tf_op | source)
XLA Modules:
  0.0 117.1 jit_solution(1551921632175454042)
XLA Ops:
  0.0 1.4 %copy.11.taps = f32[2,3,1408]{2,1,0:T(4,128)} copy(f32[2,3,1408]{2,0,1:T(2,128)} %param.18) | data formatting | bytes 67584 | tf_op args[8]
  1.4 113.5 %shard_map.100 = bf16[512,1024]{1,0:T(8,128)(2,1)} custom-call(bf16[512,1024]{1,0:T(8,128)(2,1)} %tok.1, f32[2,1024,1408]{2,1,0:T(8,128)} %gw_hbm.1, f32[2,1024,1408]{2,1,0:T(8,128)} %uw_hbm.1, f32[2,1408,1024]{2,1,0:T(8,128)} %dw_hbm.1, f32[2,1408]{1,0:T(2,128)} %gs.1, f32[2,1408]{1,0:T(2,128)} %us.1, f32[2,1024]{1,0:T(2,128)} %ds_.1, f32[2,1024]{1,0:T(2,128)} %gain.1, ...), custom_call_target="tpu_custom_call" | custom-call | tf_op jit(solution)/shard_map/pallas_call | solution.py:482
  114.9 2.3 %copy.13 = bf16[512,1024]{1,0:T(8,128)(2,1)} copy(bf16[512,1024]{1,0:T(8,128)(2,1)} %shard_map.100) | data formatting | bytes 2097152

commit v2 on v1

v2 whole, which is shorter than its diff:
```python
import functools

import jax
import jax.numpy as jnp
from jax import lax
from jax.experimental import pallas as pl
from jax.experimental.pallas import tpu as pltpu
from jax.sharding import PartitionSpec as P

MESH = pl.DeviceIdType.MESH
norm_eps = 1e-06
residual_scale = 0.25
LANES = 128
PACK = 16


ENDS = ((2, 3, 4, 6, 7, 8), (1, 2, 3, 5, 7, 8))


def row_chunks(n_tok):
    return [[(a * n_tok // 8, b * n_tok // 8) for a, b in zip((0,) + ends[:-1], ends)] for ends in ENDS]


ORDER = (
    ("M", 0, 0), ("G", 0, 0), ("K", 0, 0), ("A", 0, 0), ("B", 0, 0), ("G", 0, 1), ("K", 0, 1), ("G", 0, 2),
    ("C", 0, 0), ("A", 0, 1), ("K", 0, 2), ("H", 0, 0), ("B", 0, 1), ("G", 0, 3), ("I", 0, 0), ("A", 0, 2),
    ("H", 0, 1), ("K", 0, 3), ("F", 0, 0), ("B", 0, 2), ("G", 0, 4), ("J", 0, 0), ("I", 0, 1), ("A", 0, 3),
    ("D", 0, 0), ("H", 0, 2), ("F", 0, 1), ("B", 0, 3), ("K", 0, 4), ("J", 0, 1), ("A", 0, 4), ("I", 0, 2),
    ("G", 0, 5), ("D", 0, 1), ("F", 0, 2), ("Z", 0, 0), ("H", 0, 3), ("I", 0, 3), ("A", 0, 5), ("K", 0, 5),
    ("Z", 0, 1), ("J", 0, 2), ("F", 0, 3), ("B", 0, 4), ("B", 0, 5), ("C", 1, 0), ("D", 0, 2), ("J", 0, 3),
    ("E", 0, 0), ("H", 0, 5), ("D", 0, 3), ("E", 0, 1), ("H", 0, 4), ("I", 0, 5), ("Z", 0, 2), ("F", 0, 5),
    ("I", 0, 4), ("W", 0, 0), ("J", 0, 5), ("Z", 0, 3), ("D", 0, 5), ("F", 0, 4), ("J", 0, 4), ("W", 0, 1),
    ("E", 0, 2), ("D", 0, 4), ("N", 0, 0), ("Z", 0, 5), ("E", 0, 3), ("M", 1, 0), ("W", 0, 2), ("R", 0, 0),
    ("Z", 0, 4), ("G", 1, 0), ("N", 0, 1), ("K", 1, 0), ("A", 1, 0), ("N", 0, 2), ("E", 0, 5), ("R", 0, 1),
    ("B", 1, 0), ("W", 0, 3), ("G", 1, 1), ("K", 1, 1), ("E", 0, 4), ("A", 1, 1), ("R", 0, 2), ("G", 1, 2),
    ("H", 1, 0), ("W", 0, 5), ("I", 1, 0), ("N", 0, 3), ("A", 1, 2), ("K", 1, 2), ("B", 1, 1), ("W", 0, 4),
    ("F", 1, 0), ("H", 1, 1), ("B", 1, 2), ("N", 0, 5), ("R", 0, 3), ("G", 1, 3), ("J", 1, 0), ("H", 1, 2),
    ("N", 0, 4), ("A", 1, 3), ("K", 1, 3), ("R", 0, 5), ("I", 1, 2), ("F", 1, 2), ("F", 1, 1), ("I", 1, 1),
    ("B", 1, 3), ("R", 0, 4), ("G", 1, 4), ("K", 1, 4), ("A", 1, 4), ("J", 1, 2), ("D", 1, 0), ("H", 1, 3),
    ("B", 1, 4), ("D", 1, 2), ("J", 1, 1), ("D", 1, 1), ("Z", 1, 0), ("I", 1, 3), ("G", 1, 5), ("H", 1, 4),
    ("F", 1, 3), ("Z", 1, 2), ("K", 1, 5), ("I", 1, 4), ("A", 1, 5), ("Z", 1, 1), ("J", 1, 3), ("E", 1, 0),
    ("F", 1, 4), ("B", 1, 5), ("D", 1, 3), ("E", 1, 2), ("J", 1, 4), ("E", 1, 1), ("H", 1, 5), ("D", 1, 4),
    ("I", 1, 5), ("Z", 1, 3), ("F", 1, 5), ("W", 1, 1), ("Z", 1, 4), ("W", 1, 2), ("J", 1, 5), ("D", 1, 5),
    ("E", 1, 3), ("W", 1, 0), ("N", 1, 1), ("Z", 1, 5), ("E", 1, 4), ("W", 1, 3), ("E", 1, 5), ("N", 1, 2),
    ("W", 1, 4), ("W", 1, 5), ("N", 1, 4), ("N", 1, 3), ("N", 1, 0), ("N", 1, 5),
)

def kernel(
    sizes,
    tok,
    gw_hbm,
    uw_hbm,
    dw_hbm,
    gs,
    us,
    ds_,
    gain,
    taps,
    bias,
    out,
    gw,
    uw,
    dw,
    dwb,
    operand,
    rsb,
    stat,
    part,
    crecv,
    xsend,
    xrecv,
    hid,
    ysend,
    own,
    yrecv,
    zsend,
    zrecv,
    hnew,
    raw,
    wsem,
    lsem,
    ssem,
    sent,
    csem,
    xsem,
    hsem,
    osem,
    ysem,
    zsem,
    asem,
    fsem,
):
    chunks, n_tok, d_loc, f_loc, d_all, n_z = sizes
    layers = len(chunks)
    tiles = f_loc // LANES
    units = (tiles + 1) // 2
    pairs, middle = tiles // 2, units // 2
    piece, d_half = d_loc // (2 * n_z), d_loc // 2
    first = [sum(len(c) for c in chunks[:l]) for l in range(layers)]
    f32, bf16 = jnp.float32, jnp.bfloat16
    ra, cb = lax.axis_index("ra"), lax.axis_index("cb")
    z, y = ra // 2, ra % 2
    x, c = cb // 2, cb % 2
    core_dev = (ra, x * 2 + (1 - c))
    x_dev = (ra, (1 - x) * 2 + c)
    y_dev = (z * 2 + (1 - y), cb)

    def z_dev(i):
        return (lax.rem(z + i, n_z) * 2 + y, cb)

    def remote(src, dst, sems, dev):
        return pltpu.make_async_remote_copy(
            src_ref=src, dst_ref=dst, send_sem=sems[0], recv_sem=sems[1], device_id=dev, device_id_type=MESH
        )

    def span_of(at, width, size=1):
        return pl.ds(pl.multiple_of(at * width, width), size * width)

    def each(fn, begin=0, end=units):
        stop = min(end, pairs)
        if stop > begin:

            def step(u, carry):
                fn(u, 2)
                return carry

            lax.fori_loop(begin, stop, step, 0)
        if end > pairs:
            fn(pairs, 1)

    def first_load(u, w, n):
        src, dst = ((gw_hbm, gw), (uw_hbm, uw))[n]
        cols = span_of(u * 2, LANES, w)
        return pltpu.make_async_copy(src.at[0, :, cols], dst.at[0, :, cols], wsem.at[u, n])

    def load(l, n):
        src, dst = ((gw_hbm, gw), (uw_hbm, uw), (dw_hbm, dw))[n]
        return pltpu.make_async_copy(src.at[l], dst if n == 2 else dst.at[l], lsem.at[l, n])

    def start_first(u, w):
        first_load(u, w, 0).start()
        first_load(u, w, 1).start()

    each(start_first)

    def stat_copy(n, k):
        return remote(stat.at[n, 0], stat.at[n, k], (ssem.at[0, n], ssem.at[1, n]), (ra, lax.rem(cb + k, 4)))

    def picked(s, e):
        lane = lax.broadcasted_iota(jnp.int32, (e - s, LANES), 1)
        row = lax.broadcasted_iota(jnp.int32, (e - s, LANES), 0)
        return lane == lax.shift_right_logical(row + s, 3)

    def squares(n, h, l, s, e):
        wide = h[s:e, :].astype(f32)
        ssq = jnp.sum(wide * wide, axis=1, keepdims=True)
        packed = jnp.where(picked(s, e), jnp.broadcast_to(ssq, (e - s, LANES)), 0.0)
        stat[n, 0] = jnp.sum(packed.reshape((e - s) // 8, 8, LANES), axis=0)
        operand[s:e, :] = (wide * gain[l : l + 1, :]).astype(bf16)

    def share_squares(n):
        for k in range(1, 4):
            stat_copy(n, k).start()

    def scale_rows(n, s, e):
        others = stat.at[n, 1:4]
        remote(others, others, (ssem.at[0, n], ssem.at[1, n]), core_dev).wait()
        total = stat[n, 0] + stat[n, 1] + stat[n, 2] + stat[n, 3]
        spread = jnp.broadcast_to(total[None], ((e - s) // 8, 8, LANES)).reshape(e - s, LANES)
        summed = jnp.sum(jnp.where(picked(s, e), spread, 0.0), axis=1, keepdims=True)
        rsb[s:e, :] = jnp.broadcast_to(lax.rsqrt(summed / d_all + norm_eps), (e - s, LANES))

    def cast_down(l):
        load(l, 2).wait()

        def step(i, carry):
            r = span_of(i, LANES)
            dwb[l, r, :] = dw[r, :].astype(bf16)
            return carry

        lax.fori_loop(0, tiles, step, 0)
        if l + 1 < layers:
            load(l + 1, 2).start()

    def wait_sent(l, n):
        block = (
            part.at[0 : n_tok // 2, :],
            xsend,
            hid.at[l, 0 : 3 * n_tok // 4, :],
            ysend,
            zsend.at[:, 0 : (n_z - 1) * piece],
            hnew.at[l, :, 0 : (n_z - 1) * piece],
            hnew.at[l, :, 0:d_half],
        )[n]
        remote(block, block, (sent.at[l, n], csem.at[0, 0]), core_dev).wait_send()

    def steps_of(l, k):
        s, e = chunks[l][k]
        at = first[l] + k
        half, quarter = (e - s) // 2, (e - s) // 4
        lo, hi = max(s - PACK, 0), min(e + PACK, n_tok)
        h = tok if l == 0 else hnew.at[l - 1]

        def block_rows(cc, xx):
            return pl.ds(pl.multiple_of(s + cc * half + xx * quarter, PACK), quarter)

        def local_rows(xx):
            return pl.ds(pl.multiple_of(s // 2 + xx * quarter, PACK), quarter)

        x_rows = slice(s // 4, e // 4)

        def wide_cols(hf, width):
            return slice(0, middle * width) if hf == 0 else slice(middle * width, 2 * f_loc * width // (4 * LANES))

        def core_copy(hf):
            rows = pl.ds(pl.multiple_of(s + (1 - c) * half, PACK), half)
            cols = wide_cols(hf, 4 * LANES)
            return remote(part.at[rows, cols], crecv.at[l, s // 2 : e // 2, cols], (sent.at[l, 0], csem.at[at, hf]), core_dev)

        def x_copy(hf):
            cols = wide_cols(hf, 4 * LANES)
            return remote(xsend.at[x_rows, cols], xrecv.at[l, x_rows, cols], (sent.at[l, 1], xsem.at[at, hf]), x_dev)

        def h_copy(hf, n):
            block = hid.at[l, block_rows(c, 1 - x if n == 2 else x), wide_cols(hf, 2 * LANES)]
            return remote(block, block, (sent.at[l, 2], hsem.at[at, hf] if n == 0 else osem.at[at]), x_dev if n == 0 else core_dev)

        def y_copy(i):
            cols = span_of(lax.rem(z + i, n_z), piece)
            return remote(ysend.at[s:e, cols], yrecv.at[l, s:e, cols], (sent.at[l, 3], ysem.at[at, i - 1]), y_dev)

        def z_copy(i):
            cols = span_of(lax.rem(z + i, n_z), piece)
            return remote(zsend.at[s:e, cols], zrecv.at[l, i - 1, s:e, :], (sent.at[l, 4], zsem.at[at]), z_dev(i))

        def gather_z(i):
            block = hnew.at[l, s:e, span_of(y * n_z + z, piece)]
            return remote(block, block, (sent.at[l, 5], asem.at[at, i - 1]), z_dev(i))

        def gather_y(i):
            block = hnew.at[l, s:e, span_of(y * n_z + lax.rem(z + n_z - i, n_z), piece)]
            return remote(block, block, (sent.at[l, 6], fsem.at[at]), y_dev)

        def product(u, w):
            cols = span_of(u * 2, LANES, w)
            weights = jnp.concatenate([gw[l, :, cols].astype(bf16), uw[l, :, cols].astype(bf16)], axis=1)
            return jnp.dot(operand[lo:hi, :], weights, preferred_element_type=f32)

        def raw_unit(u, w):
            if l == 0:
                first_load(u, w, 0).wait()
                first_load(u, w, 1).wait()
            raw[0 : hi - lo, span_of(u * 4, LANES, 2 * w)] = product(u, w)

        def gate_unit(u, w):
            acc = raw[0 : hi - lo, span_of(u * 4, LANES, 2 * w)] if k == 0 else product(u, w)
            rs = rsb[lo:hi, :]
            rows = lax.broadcasted_iota(jnp.int32, rs.shape, 0)
            for i in range(w):
                col = span_of(u * 2 + i, LANES)
                g = acc[:, i * LANES : (i + 1) * LANES] * rs * gs[l : l + 1, col]
                prev, nxt = pltpu.roll(g, 1, 0), pltpu.roll(g, hi - lo - 1, 0)
                if s == 0:
                    prev = jnp.where(rows == 0, 0.0, prev)
                if e == n_tok:
                    nxt = jnp.where(rows == hi - lo - 1, 0.0, nxt)
                mixed = taps[0, l : l + 1, col] * prev + taps[1, l : l + 1, col] * g + taps[2, l : l + 1, col] * nxt
                upward = acc[:, (w + i) * LANES : (w + i + 1) * LANES] * rs * us[l : l + 1, col]
                part[s:e, span_of(u * 4 + 2 * i, LANES)] = mixed[s - lo : e - lo].astype(bf16)
                part[s:e, span_of(u * 4 + 2 * i + 1, LANES)] = upward[s - lo : e - lo].astype(bf16)

        def x_unit(u, w):
            cols = span_of(u * 4, LANES, 2 * w)
            mine = part[block_rows(c, 1 - x), cols].astype(f32)
            xsend[x_rows, cols] = (mine + crecv[l, local_rows(1 - x), cols].astype(f32)).astype(bf16)

        def hidden_unit(u, w):
            cols = span_of(u * 4, LANES, 2 * w)
            rows = block_rows(c, x)
            total = (
                part[rows, cols].astype(f32)
                + crecv[l, local_rows(x), cols].astype(f32)
                + xrecv[l, x_rows, cols].astype(f32)
            )
            for i in range(w):
                col = span_of(u * 2 + i, LANES)
                mixed = total[:, 2 * i * LANES : (2 * i + 1) * LANES] + bias[l : l + 1, col]
                upward = total[:, (2 * i + 1) * LANES : (2 * i + 2) * LANES]
                hid[l, rows, col] = (mixed / (1.0 + jnp.exp(-mixed)) * upward).astype(bf16)

        def bounds(hf):
            return (0, middle) if hf == 0 else (middle, units)

        def gate(hf):
            each(gate_unit, *bounds(hf))
            core_copy(hf).start()

        def reduce_x(hf):
            core_copy(hf).wait_recv()
            each(x_unit, *bounds(hf))
            x_copy(hf).start()

        def hidden(hf):
            x_copy(hf).wait_recv()
            each(hidden_unit, *bounds(hf))
            h_copy(hf, 0).start()
            h_copy(hf, 1).start()

        def forward_hidden(hf):
            h_copy(hf, 0).wait_recv()
            h_copy(hf, 2).start()

        def down():
            theirs = hid.at[l, pl.ds(pl.multiple_of(s + (1 - c) * half, PACK), half), :]
            remote(theirs, theirs, (sent.at[l, 2], osem.at[at]), core_dev).wait_recv()
            rows = hid[l, s:e, :]
            other = jnp.dot(rows, dwb[l, :, span_of(1 - y, d_half)], preferred_element_type=f32)
            ysend[s:e, :] = other.astype(bf16)
            for i in range(1, n_z + 1):
                y_copy(i).start()
            own[s:e, :] = jnp.dot(rows, dwb[l, :, span_of(y, d_half)], preferred_element_type=f32)

        def spread():
            for i in range(1, n_z):
                cols = span_of(lax.rem(z + i, n_z), piece)
                y_copy(i).wait_recv()
                zsend[s:e, cols] = (own[s:e, cols] + yrecv[l, s:e, cols].astype(f32)).astype(bf16)
                z_copy(i).start()

        def finish():
            cols, mine = span_of(z, piece), span_of(y * n_z + z, piece)
            y_copy(n_z).wait_recv()
            acc = own[s:e, cols] + yrecv[l, s:e, cols].astype(f32)
            pieces = zrecv.at[l, :, s:e, :]
            remote(pieces, pieces, (sent.at[l, 4], zsem.at[at]), y_dev).wait_recv()
            for i in range(1, n_z):
                acc = acc + zrecv[l, i - 1, s:e, :].astype(f32)
            new = residual_scale * h[s:e, mine].astype(f32) + acc * ds_[l : l + 1, mine]
            hnew[l, s:e, mine] = new.astype(bf16)
            for i in range(1, n_z):
                gather_z(i).start()
            gather_y(0).start()

        def forward():
            for i in range(1, n_z):
                gather_z(i).wait_recv()
                gather_y(i).start()

        def arrived():
            theirs = hnew.at[l, s:e, span_of(1 - y, d_half)]
            remote(theirs, theirs, (sent.at[l, 6], fsem.at[at]), y_dev).wait_recv()
            if l + 1 < layers:
                squares(1 + at, hnew.at[l], l + 1, s, e)
                share_squares(1 + at)
            else:
                out[s:e, :] = hnew[l, s:e, :]

        return {
            "M": functools.partial(each, raw_unit),
            "G": functools.partial(gate, 0),
            "K": functools.partial(gate, 1),
            "A": functools.partial(reduce_x, 0),
            "B": functools.partial(reduce_x, 1),
            "H": functools.partial(hidden, 0),
            "I": functools.partial(hidden, 1),
            "F": functools.partial(forward_hidden, 0),
            "J": functools.partial(forward_hidden, 1),
            "D": down,
            "Z": spread,
            "E": finish,
            "W": forward,
            "N": arrived,
            "R": functools.partial(scale_rows, 1 + at, s, e),
            "C": functools.partial(cast_down, l),
        }

    squares(0, tok, 0, 0, n_tok)
    barrier = pltpu.get_barrier_semaphore()
    peers = [(ra, lax.rem(cb + k, 4)) for k in range(1, 4)] + [y_dev] + [z_dev(k) for k in range(1, n_z)]
    for dev in peers:
        pl.semaphore_signal(barrier, inc=1, device_id=dev, device_id_type=MESH)
    pl.semaphore_wait(barrier, len(peers))

    share_squares(0)
    steps = {(l, k): steps_of(l, k) for l in range(layers) for k in range(len(chunks[l]))}
    begun = set()
    reused = {"G": 0, "A": 1, "D": 3, "Z": 4}
    for s, l, k in ORDER:
        if l > 0 and (s, l) not in begun and s in reused:
            wait_sent(l - 1, reused[s])
        begun.add((s, l))
        if s == "M" and l > 0:
            load(l, 0).wait()
            load(l, 1).wait()
        steps[l, k][s]()
        if (s, l) == ("M", 0):
            load(0, 2).start()
            for ll in range(1, layers):
                load(ll, 0).start()
                load(ll, 1).start()
            scale_rows(0, 0, n_tok)
    for l in range(layers):
        for n in range(7):
            if l == layers - 1 or n not in reused.values():
                wait_sent(l, n)


def fused(n_ra, tokens, gate_weight, up_weight, down_weight, gate_scale, up_scale, down_scale, gain, taps, bias, d_all):
    n_tok, d_loc = tokens.shape
    layers, _, f_loc = gate_weight.shape
    n_z = n_ra // 2
    chunks = row_chunks(n_tok)
    total = sum(len(c) for c in chunks)
    tiles = f_loc // LANES
    units = (tiles + 1) // 2
    f32, bf16 = jnp.float32, jnp.bfloat16
    dma = pltpu.SemaphoreType.DMA
    vmem, hbm = pl.BlockSpec(memory_space=pltpu.VMEM), pl.BlockSpec(memory_space=pl.ANY)
    return pl.pallas_call(
        functools.partial(kernel, (chunks, n_tok, d_loc, f_loc, d_all, n_z)),
        out_shape=jax.ShapeDtypeStruct((n_tok, d_loc), bf16),
        in_specs=[vmem, hbm, hbm, hbm] + [vmem] * 6,
        out_specs=vmem,
        scratch_shapes=[
            pltpu.VMEM((layers, d_loc, f_loc), f32),
            pltpu.VMEM((layers, d_loc, f_loc), f32),
            pltpu.VMEM((f_loc, d_loc), f32),
            pltpu.VMEM((layers, f_loc, d_loc), bf16),
            pltpu.VMEM((n_tok, d_loc), bf16),
            pltpu.VMEM((n_tok, LANES), f32),
            pltpu.VMEM((1 + total, 4, 8, LANES), f32),
            pltpu.VMEM((n_tok, 2 * f_loc), bf16),
            pltpu.VMEM((layers, n_tok // 2, 2 * f_loc), bf16),
            pltpu.VMEM((n_tok // 4, 2 * f_loc), bf16),
            pltpu.VMEM((layers, n_tok // 4, 2 * f_loc), bf16),
            pltpu.VMEM((layers, n_tok, f_loc), bf16),
            pltpu.VMEM((n_tok, d_loc // 2), bf16),
            pltpu.VMEM((n_tok, d_loc // 2), f32),
            pltpu.VMEM((layers, n_tok, d_loc // 2), bf16),
            pltpu.VMEM((n_tok, d_loc // 2), bf16),
            pltpu.VMEM((layers, n_z - 1, n_tok, d_loc // n_ra), bf16),
            pltpu.VMEM((layers, n_tok, d_loc), bf16),
            pltpu.VMEM((chunks[0][0][1] + PACK, 2 * f_loc), f32),
            dma((units, 2)),
            dma((layers, 3)),
            dma((2, 1 + total)),
            dma((layers, 7)),
            dma((total, 2)),
            dma((total, 2)),
            dma((total, 2)),
            dma((total,)),
            dma((total, n_z)),
            dma((total,)),
            dma((total, n_z - 1)),
            dma((total,)),
        ],
        compiler_params=pltpu.CompilerParams(
            collective_id=0, has_side_effects=True, vmem_limit_bytes=67_043_328
        ),
    )(tokens, gate_weight, up_weight, down_weight, gate_scale, up_scale, down_scale, gain, jnp.transpose(taps, (1, 0, 2)), bias)


def plain(tokens, gate_weight, up_weight, down_weight, gate_scale, up_scale, down_scale, gain, conv_taps, bias, d_all):
    hstate = tokens
    for layer in range(gate_weight.shape[0]):
        wide = hstate.astype(jnp.float32)
        squares = jnp.sum(wide * wide, axis=1)
        operand = (wide * gain[layer]).astype(jnp.bfloat16)
        gate_part = jnp.dot(operand, gate_weight[layer].astype(jnp.bfloat16), preferred_element_type=jnp.float32)
        up_part = jnp.dot(operand, up_weight[layer].astype(jnp.bfloat16), preferred_element_type=jnp.float32)
        gate_sum, up_sum, square_sum = lax.psum((gate_part, up_part, squares), "cb")
        rscale = lax.rsqrt(square_sum / d_all + norm_eps)[:, None]
        gate = gate_sum * rscale * gate_scale[layer]
        upward = up_sum * rscale * up_scale[layer]
        padded = jnp.pad(gate, ((1, 1), (0, 0)))
        taps = conv_taps[layer]
        mixed = taps[0] * padded[:-2] + taps[1] * padded[1:-1] + taps[2] * padded[2:] + bias[layer]
        hidden = (jax.nn.silu(mixed) * upward).astype(jnp.bfloat16)
        term = jnp.dot(hidden, down_weight[layer].astype(jnp.bfloat16), preferred_element_type=jnp.float32)
        branch = lax.psum(term, "ra") * down_scale[layer]
        hstate = (residual_scale * wide + branch).astype(jnp.bfloat16)
    return hstate


def solution(mesh):
    n_ra, n_cb = mesh.shape["ra"], mesh.shape["cb"]

    def per_device(*args):
        n_tok, d_loc = args[0].shape
        f_loc = args[1].shape[2]
        fits = n_cb == 4 and n_ra % 2 == 0 and n_ra >= 4 and n_tok % (8 * 4 * PACK) == 0 and n_tok <= 8 * LANES
        fits = fits and f_loc % LANES == 0 and d_loc % (LANES * n_ra) == 0 and f_loc >= 4 * LANES and args[1].shape[0] == len(ENDS)
        if fits:
            return fused(n_ra, *args, d_loc * n_cb)
        return plain(*args, d_loc * n_cb)

    in_specs = (
        P(None, "cb"),
        P(None, "cb", "ra"),
        P(None, "cb", "ra"),
        P(None, "ra", "cb"),
        P(None, "ra"),
        P(None, "ra"),
        P(None, "cb"),
        P(None, "cb"),
        P(None, None, "ra"),
        P(None, "ra"),
    )
    return jax.shard_map(
        per_device, mesh=mesh, in_specs=in_specs, out_specs=P(None, "cb"), check_vma=False
    )
```

time: 117 us -> 102 us (0.87)
  Pallas kernels: 113 us -> 99.2 us
  local copies, waits for them, and re-layouts: 3.65 us -> 2.26 us
    pallas_call x1, Pallas kernels: 113 us -> 99.2 us  [fused(): pl.pallas_call(functools.partial(kernel, (chunks, n_tok, d_loc, f_loc, d_...]
    unnamed x2 -> x1, local copies, waits for them, and re-layouts: 3.65 us -> 2.26 us
where the time goes in v2:
time: 102 us
  Pallas kernels  99.2 us (97%)
  local copies, waits for them, and re-layouts  2.26 us (2%)
    pallas_call x1, Pallas kernels, fused(): pl.pallas_call(functools.partial(kernel, (chunks, n_tok, d_loc, f_loc, d_...  99.2 us
    unnamed x1, local copies, waits for them, and re-layouts  2.26 us

profile of v2, /device:TPU:0, one launch (start us, length us, event | category | flops | bytes accessed | tf_op | source)
XLA Modules:
  0.0 101.5 jit_solution(14383219926473853917)
XLA Ops:
  0.0 99.2 %shard_map.100 = bf16[512,1024]{1,0:T(8,128)(2,1)} custom-call(bf16[512,1024]{1,0:T(8,128)(2,1)} %tok.1, f32[2,1024,1408]{2,1,0:T(8,128)} %gw_hbm.1, f32[2,1024,1408]{2,1,0:T(8,128)} %uw_hbm.1, f32[2,1408,1024]{2,1,0:T(8,128)} %dw_hbm.1, f32[2,1408]{1,0:T(2,128)} %gs.1, f32[2,1408]{1,0:T(2,128)} %us.1, f32[2,1024]{1,0:T(2,128)} %ds_.1, f32[2,1024]{1,0:T(2,128)} %gain.1, ...), custom_call_target="tpu_custom_call" | custom-call | tf_op jit(solution)/shard_map/pallas_call | solution.py:419
  99.2 2.3 %copy.12 = bf16[512,1024]{1,0:T(8,128)(2,1)} copy(bf16[512,1024]{1,0:T(8,128)(2,1)} %shard_map.100) | data formatting | bytes 2097152

commit v3 on v2

--- a/solution.py
+++ b/solution.py
@@ -374,11 +374,11 @@
             "C": functools.partial(cast_down, l),
         }
 
-    squares(0, tok, 0, 0, n_tok)
     barrier = pltpu.get_barrier_semaphore()
     peers = [(ra, lax.rem(cb + k, 4)) for k in range(1, 4)] + [y_dev] + [z_dev(k) for k in range(1, n_z)]
     for dev in peers:
         pl.semaphore_signal(barrier, inc=1, device_id=dev, device_id_type=MESH)
+    squares(0, tok, 0, 0, n_tok)
     pl.semaphore_wait(barrier, len(peers))
 
     share_squares(0)
@@ -418,7 +418,7 @@
     vmem, hbm = pl.BlockSpec(memory_space=pltpu.VMEM), pl.BlockSpec(memory_space=pl.ANY)
     return pl.pallas_call(
         functools.partial(kernel, (chunks, n_tok, d_loc, f_loc, d_all, n_z)),
-        out_shape=jax.ShapeDtypeStruct((n_tok, d_loc), bf16),
+        out_shape=pltpu.VMEM((n_tok, d_loc), bf16),
         in_specs=[vmem, hbm, hbm, hbm] + [vmem] * 6,
         out_specs=vmem,
         scratch_shapes=[
@@ -455,7 +455,7 @@
             dma((total,)),
         ],
         compiler_params=pltpu.CompilerParams(
-            collective_id=0, has_side_effects=True, vmem_limit_bytes=67_043_328
+            collective_id=0, has_side_effects=True, vmem_limit_bytes=60_000_000
         ),
     )(tokens, gate_weight, up_weight, down_weight, gate_scale, up_scale, down_scale, gain, jnp.transpose(taps, (1, 0, 2)), bias)
 

time: 102 us -> 99.2 us (0.973)
  local copies, waits for them, and re-layouts: 2.26 us -> 0.97 us
  Pallas kernels: 99.2 us -> 98.1 us
    unnamed x1, local copies, waits for them, and re-layouts: 2.26 us -> 0.97 us
    pallas_call x1, Pallas kernels: 99.2 us -> 98.1 us  [fused(): pl.pallas_call(functools.partial(kernel, (chunks, n_tok, d_loc, f_loc, d_...]
where the time goes in v3:
time: 99.2 us; the launch traced here: 99.1 us
  Pallas kernels  98.1 us (99%)
    pallas_call x1, Pallas kernels, fused(): pl.pallas_call(functools.partial(kernel, (chunks, n_tok, d_loc, f_loc, d_...  98.1 us

profile of v3, /device:TPU:0, one launch (start us, length us, event | category | flops | bytes accessed | tf_op | source)
XLA Modules:
  0.0 99.1 jit_solution(1077193242592289872)
XLA Ops:
  0.0 98.1 %shard_map.100 = bf16[512,1024]{1,0:T(8,128)(2,1)S(1)} custom-call(bf16[512,1024]{1,0:T(8,128)(2,1)} %tok.1, f32[2,1024,1408]{2,1,0:T(8,128)} %gw_hbm.1, f32[2,1024,1408]{2,1,0:T(8,128)} %uw_hbm.1, f32[2,1408,1024]{2,1,0:T(8,128)} %dw_hbm.1, f32[2,1408]{1,0:T(2,128)} %gs.1, f32[2,1408]{1,0:T(2,128)} %us.1, f32[2,1024]{1,0:T(2,128)} %ds_.1, f32[2,1024]{1,0:T(2,128)} %gain.1, ...), custom_call_target="tpu_custom_call" | custom-call | tf_op jit(solution)/shard_map/pallas_call | solution.py:419
  98.1 1.0 copy.12
